TPU v7x, 32 devices: a whole 2x2x4 slice. The times are simulated.
32 devices in a mesh: sp: 4 (over z), fs: 4 (over y, x), tp: 2 (over core).
Axes of the slice: x: 2, y: 2, z: 4, core: 2. Of those that a mesh axis runs over, the one named last changes fastest.
Arguments:
- tokens: bfloat16 [4, 1024, 2048], P('fs', 'sp', 'tp'), may hold values from -6 to 6
- norm_gain: float32 [2048], replicated, may hold values from 0.1 to 1.9
- w_query: bfloat16 [2048, 1024], P(('sp', 'fs'), 'tp'), may hold values from -0.125 to 0.125
- forget_weight: bfloat16 [2048, 1024], P(('sp', 'fs'), 'tp'), may hold values from -0.125 to 0.125
- w_input: bfloat16 [2048, 1024], P(('sp', 'fs'), 'tp'), may hold values from -8 to 8
- w_outgate: bfloat16 [2048, 1024], P(('sp', 'fs'), 'tp'), may hold values from -0.125 to 0.125
- w_pool: bfloat16 [2048, 1024], P(('sp', 'fs'), 'tp'), may hold values from -0.125 to 0.125
- forget_gap: float32 [1024], P('tp'), may hold values from 0 to 0.07
- extra_decay: float32 [4, 1024, 8], P('fs', 'sp', 'tp'), may hold values from -0.61 to 0
- rec_gain: float32 [1024], P('tp'), may hold values from 0.1 to 1.9
- group_weight: bfloat16 [4, 256, 256], replicated, may hold values from -0.375 to 0.375
- pool_gain: float32 [1024], P('tp'), may hold values from 0.1 to 1.9
- recurrent_output_weight: bfloat16 [1024, 2048], P('tp', ('sp', 'fs')), may hold values from -0.1875 to 0.1875
- w_out_pool: bfloat16 [1024, 2048], P('tp', ('sp', 'fs')), may hold values from -0.1875 to 0.1875
Outputs:
- mixed_out: bfloat16 [4, 1024, 2048], P('fs', ('sp', 'tp'))
All inputs are finite; a program needn't handle non-finite values.
Results may differ from a plain program's by a relative error of at most 0.011.
Values may be sent and summed in bfloat16 or wider, within the bound.
A program may use at most 64 MiB of HBM per device.

v0:
```python
import jax
import jax.numpy as jnp
from jax import lax
from jax.sharding import PartitionSpec as P

HEAD_DIM = 128
D_HGRN = 1024
POOL_GROUPS = 4
GROUP_DIM = 256
BLOCK = 64
EPS = 1e-06
HIGH = lax.Precision.HIGHEST


def carried_in(x, axis, join, neutral):
    place = lax.axis_index(axis)
    gathered = jax.tree.map(
        lambda a, kind: lax.all_gather(a.astype(kind), axis), x, (jnp.bfloat16, jnp.bfloat16)
    )
    state = jax.tree.map(lambda a, e: jnp.zeros_like(a) + jnp.asarray(e, a.dtype), x, neutral)

    def one(lap, state):
        return join(
            state,
            jax.tree.map(
                lambda a, own: lax.dynamic_index_in_dim(a, lap, 0, False).astype(own.dtype),
                gathered,
                x,
            ),
        )

    return lax.fori_loop(0, place, one, state)


def shifted(x, axis, by):
    peers = lax.axis_size(axis)
    pairs = [(i, i + by) for i in range(peers) if 0 <= i + by < peers]
    return lax.ppermute(x, axis, pairs)


def local_recurrence(queries, input_gate, values, log_forget):
    tok_rows, head_count = (queries.shape[0], queries.shape[1])
    block_count = tok_rows // BLOCK
    q_blk, k_blk, v_blk, g_blk = (
        arr.reshape(block_count, BLOCK, head_count, HEAD_DIM)
        for arr in (queries, input_gate, values, log_forget)
    )
    within = jnp.cumsum(g_blk, axis=1)
    block_end = within[:, -1]
    q_up = q_blk * jnp.exp(within)
    k_down = k_blk * jnp.exp(-within)
    causal = jnp.tril(jnp.ones((BLOCK, BLOCK), jnp.bool_))
    scores = jnp.einsum("nthd,nshd->nhts", q_up, k_down, precision=HIGH)
    scores = jnp.where(causal, scores, 0.0)
    inner_out = jnp.einsum("nhts,nshe->nthe", scores, v_blk, precision=HIGH)
    updates = jnp.einsum(
        "nshd,nshe->nhde", k_blk * jnp.exp(block_end[:, None] - within), v_blk, precision=HIGH
    )
    decays = jnp.exp(block_end)

    def carry_step(carried_state, step_inputs):
        current_shrink_factor, update_now = step_inputs
        return (current_shrink_factor[:, :, None] * carried_state + update_now, carried_state)

    zero_state = jnp.zeros((head_count, HEAD_DIM, HEAD_DIM), jnp.float32)
    final_state, incoming = lax.scan(carry_step, zero_state, (decays, updates))
    local_out = inner_out + jnp.einsum("nthd,nhde->nthe", q_up, incoming, precision=HIGH)
    offsets = jnp.cumsum(block_end, axis=0) - block_end
    total_log = jnp.sum(block_end, axis=0)
    query_dev = q_up * jnp.exp(offsets[:, None])
    return (local_out, final_state, total_log, query_dev)


def combine_states(earlier, later):
    decay_early, state_early = earlier
    decay_late, state_late = later
    return (decay_early * decay_late, decay_late[:, :, None] * state_early + state_late)


def body(
    tokens,
    norm_gain,
    w_query,
    forget_weight,
    w_input,
    w_outgate,
    w_pool,
    forget_gap,
    extra_decay,
    rec_gain,
    group_weight,
    pool_gain,
    recurrent_output_weight,
    w_out_pool,
):
    gathered = lax.all_gather(tokens[0], "tp", axis=1, tiled=True)
    features_f = gathered.astype(jnp.float32)
    token_scale = lax.rsqrt(jnp.mean(features_f * features_f, axis=-1, keepdims=True) + EPS)
    normed = (features_f * token_scale * norm_gain).astype(jnp.bfloat16)
    tok_rows = normed.shape[0]
    width_dev = w_query.shape[1]
    pool_dev = w_pool.shape[1]
    near_rows = (
        lax.all_gather(w_query, "fs", axis=0, tiled=True),
        lax.all_gather(forget_weight, "fs", axis=0, tiled=True),
        lax.all_gather(w_input, "fs", axis=0, tiled=True),
        lax.all_gather(w_outgate, "fs", axis=0, tiled=True),
        lax.all_gather(w_pool, "fs", axis=0, tiled=True),
    )
    full_rows = (
        lax.all_gather(near_rows[0], "sp", axis=0, tiled=True),
        lax.all_gather(near_rows[1], "sp", axis=0, tiled=True),
        lax.all_gather(near_rows[2], "sp", axis=0, tiled=True),
        lax.all_gather(near_rows[3], "sp", axis=0, tiled=True),
        lax.all_gather(near_rows[4], "sp", axis=0, tiled=True),
    )
    z_query, z_forget, z_input, z_outgate, z_pool = (
        jnp.dot(normed, matrix, preferred_element_type=jnp.float32).astype(jnp.bfloat16)
        for matrix in full_rows
    )
    heads_dev = width_dev // HEAD_DIM
    input_gate = forget_gap * jax.nn.sigmoid(-z_forget.astype(jnp.float32))
    log_forget = (
        jnp.log1p(-input_gate).reshape(tok_rows, heads_dev, HEAD_DIM) + extra_decay[0][:, :, None]
    )
    queries = jax.nn.silu(z_query.astype(jnp.float32)).reshape(tok_rows, heads_dev, HEAD_DIM)
    values = z_input.astype(jnp.float32).reshape(tok_rows, heads_dev, HEAD_DIM)
    local_out, end_state, total_log, query_dev = local_recurrence(
        queries, input_gate.reshape(tok_rows, heads_dev, HEAD_DIM), values, log_forget
    )
    identity = (jnp.ones_like(total_log), jnp.zeros_like(end_state))
    scanned = carried_in((jnp.exp(total_log), end_state), "sp", combine_states, identity)
    incoming = scanned[1]
    carried = jnp.einsum("nthd,hde->nthe", query_dev, incoming, precision=HIGH)
    recurrent = (local_out + carried).reshape(tok_rows, width_dev)
    square_sum = lax.psum(jnp.sum(recurrent * recurrent, axis=1), "tp")
    rec_scale = lax.rsqrt(square_sum / D_HGRN + EPS)[:, None]
    recurrent_output = (
        recurrent * rec_scale * rec_gain * jax.nn.silu(z_outgate.astype(jnp.float32))
    ).astype(jnp.bfloat16)
    reach_rows = 2**POOL_GROUPS
    rim_rows = shifted(z_pool[tok_rows - reach_rows :], "sp", 1)
    extended = jnp.concatenate([rim_rows, z_pool], axis=0).astype(jnp.float32)
    running = extended
    window_sums = []
    for level_idx in range(POOL_GROUPS):
        stride = 2**level_idx
        running = running[stride:] + running[:-stride]
        window_sums.append(running[running.shape[0] - tok_rows :])
    groups_dev = pool_dev // GROUP_DIM
    stacked = jnp.stack(window_sums).reshape(POOL_GROUPS, tok_rows, groups_dev, GROUP_DIM)
    group_ids = lax.axis_index("tp") * groups_dev + jnp.arange(groups_dev, dtype=jnp.int32)
    chosen = jnp.arange(POOL_GROUPS, dtype=jnp.int32)[:, None] == group_ids[None, :]
    window_total = jnp.sum(jnp.where(chosen[:, None, :, None], stacked, 0.0), axis=0)
    symbol_indices = lax.axis_index("sp") * tok_rows + jnp.arange(tok_rows, dtype=jnp.int32)
    window_len = jnp.left_shift(jnp.int32(2), group_ids)
    counts_here = jnp.minimum(symbol_indices[:, None] + 1, window_len[None, :]).astype(jnp.float32)
    pooled = (
        window_total / counts_here[:, :, None]
        - z_pool.astype(jnp.float32).reshape(tok_rows, groups_dev, GROUP_DIM)
    ).astype(jnp.bfloat16)
    local_weight = lax.dynamic_slice_in_dim(
        group_weight, lax.axis_index("tp") * groups_dev, groups_dev, 0
    )
    mapped = jnp.einsum("tcd,cde->tce", pooled, local_weight, preferred_element_type=jnp.float32)
    pool_out = (mapped.reshape(tok_rows, pool_dev) * pool_gain).astype(jnp.bfloat16)
    rec_columns, pool_columns = (
        lax.all_gather(recurrent_output_weight, ("sp", "fs"), axis=1, tiled=True),
        lax.all_gather(w_out_pool, ("sp", "fs"), axis=1, tiled=True),
    )
    mixed = lax.psum_scatter(
        (
            jnp.dot(recurrent_output, rec_columns, preferred_element_type=jnp.float32)
            + jnp.dot(pool_out, pool_columns, preferred_element_type=jnp.float32)
        ).astype(jnp.bfloat16),
        "tp",
        scatter_dimension=0,
        tiled=True,
    )
    return mixed[None]


def solution(mesh):
    placed = (
        P("fs", "sp", "tp"),
        P(),
        P(("sp", "fs"), "tp"),
        P(("sp", "fs"), "tp"),
        P(("sp", "fs"), "tp"),
        P(("sp", "fs"), "tp"),
        P(("sp", "fs"), "tp"),
        P("tp"),
        P("fs", "sp", "tp"),
        P("tp"),
        P(),
        P("tp"),
        P("tp", ("sp", "fs")),
        P("tp", ("sp", "fs")),
    )
    return jax.shard_map(
        body, mesh=mesh, in_specs=placed, out_specs=P("fs", ("sp", "tp"), None), check_vma=False
    )
```

profile of v0, /device:TPU:0, one launch (start us, length us, event | category | flops | bytes accessed | tf_op | source)
XLA Modules:
  0.0 406.3 jit_solution(6593802053966810310)
XLA Ops:
  6.5 0.7 all-gather.27.cloned.1.call-update
  7.3 13.2 %all_gather.54 = bf16[512,512]{1,0:T(8,128)(2,1)} all-gather(bf16[128,512]{1,0:T(8,128)(2,1)} %param.21), channel_id=1, replica_groups=mesh['sp'=4,'fs'=4,'tp'=2] {'fs'}, dimensions={0}, use_global_device_ids=true | all-gather | bytes 655360 | tf_op jit(solution)/shard_map/all_gather | solution.py:105
  20.6 11.4 %all_gather.62 = bf16[512,512]{1,0:T(8,128)(2,1)} all-gather(bf16[128,512]{1,0:T(8,128)(2,1)} %param.24), channel_id=1, replica_groups=mesh['sp'=4,'fs'=4,'tp'=2] {'fs'}, dimensions={0}, use_global_device_ids=true | all-gather | bytes 655360 | tf_op jit(solution)/shard_map/all_gather | solution.py:108
  32.1 10.5 %all_gather.52 = bf16[512,512]{1,0:T(8,128)(2,1)} all-gather(bf16[128,512]{1,0:T(8,128)(2,1)S(1)} %copy-done.6), channel_id=1, replica_groups=mesh['sp'=4,'fs'=4,'tp'=2] {'fs'}, dimensions={0}, use_global_device_ids=true | all-gather | bytes 655360 | tf_op jit(solution)/shard_map/all_gather | solution.py:104
  42.7 10.3 %all_gather.50 = bf16[512,512]{1,0:T(8,128)(2,1)} all-gather(bf16[128,512]{1,0:T(8,128)(2,1)S(1)} %copy-done.7), channel_id=1, replica_groups=mesh['sp'=4,'fs'=4,'tp'=2] {'fs'}, dimensions={0}, use_global_device_ids=true | all-gather | bytes 655360 | tf_op jit(solution)/shard_map/all_gather | solution.py:106
  53.1 10.0 %all_gather.59 = bf16[512,512]{1,0:T(8,128)(2,1)} all-gather(bf16[128,512]{1,0:T(8,128)(2,1)S(1)} %copy-done.8), channel_id=1, replica_groups=mesh['sp'=4,'fs'=4,'tp'=2] {'fs'}, dimensions={0}, use_global_device_ids=true | all-gather | bytes 655360 | tf_op jit(solution)/shard_map/all_gather | solution.py:107
  63.2 0.7 all-gather.21.cloned.1.call-update
  63.9 0.7 all-gather.25.cloned.1.call-update
  65.7 1.5 fusion.1
  67.2 1.9 all-gather.17.cloned.1.call-done
  69.1 2.9 negate_log-plus-one_fusion
  72.5 1.2 slice_bitcast_fusion
  73.7 0.6 fusion.15
  74.4 40.8 %all-gather.23.cloned.1.call-done = bf16[2048,512]{1,0:T(8,128)(2,1)} async-done(((bf16[512,512]{1,0:T(8,128)(2,1)}), bf16[2048,512]{1,0:T(8,128)(2,1)}) %all-gather.23.cloned.1.call-update) | async-done | bytes 2097168 | tf_op jit(solution)/shard_map/all_gather | solution.py:115
  115.2 2.7 convolution_convert_fusion
  117.9 0.6 slice.57
  118.5 2.7 collective-permute-start
  121.1 1.0 reshape_reshape.11
  122.1 39.0 %all-gather.15.cloned.1.call-done = bf16[2048,512]{1,0:T(8,128)(2,1)} async-done(((bf16[512,512]{1,0:T(8,128)(2,1)}), bf16[2048,512]{1,0:T(8,128)(2,1)}) %all-gather.15.cloned.1.call-update) | async-done | bytes 2097168 | tf_op jit(solution)/shard_map/all_gather | solution.py:111
  161.1 2.4 divide_multiply_fusion
  163.5 1.1 reshape_reshape.10
  164.6 42.4 %all-gather.13.cloned.1.call-done = bf16[2048,512]{1,0:T(8,128)(2,1)} async-done(((bf16[512,512]{1,0:T(8,128)(2,1)}), bf16[2048,512]{1,0:T(8,128)(2,1)}) %all-gather.13.cloned.1.call-update) | async-done | bytes 2097168 | tf_op jit(solution)/shard_map/all_gather | solution.py:113
  207.0 2.3 convolution_convert_fusion.4
  209.4 1.7 exponential_multiply_fusion.1
  211.1 1.0 convolution_select_fusion
  212.1 1.2 fusion.39
  213.3 1.0 fusion.21
  214.3 3.7 while.26
  214.3 0.7 bitcast_dynamic-update-slice_fusion.2
  215.2 0.7 bitcast_dynamic-update-slice_fusion.2
  216.2 0.7 bitcast_dynamic-update-slice_fusion.2
  217.1 0.7 bitcast_dynamic-update-slice_fusion.2
  218.0 21.9 %all-gather.2 = bf16[16,128,128]{2,1,0:T(8,128)(2,1)S(1)} all-gather(bf16[4,128,128]{2,1,0:T(8,128)(2,1)S(1)} %convert_element_type.97), channel_id=4, replica_groups=mesh['sp'=4,'fs'=4,'tp'=2] {'sp'}, dimensions={0}, use_global_device_ids=true | all-gather | bytes 655360 | tf_op jit(solution)/shard_map/all_gather | solution.py:18
  240.0 10.1 %all-gather.3 = bf16[4,4,128]{2,1,0:T(4,128)(2,1)S(1)} all-gather(bf16[1,4,128]{2,1,0:T(4,128)(2,1)S(1)} %fusion.42), channel_id=3, replica_groups=mesh['sp'=4,'fs'=4,'tp'=2] {'sp'}, dimensions={0}, use_global_device_ids=true | all-gather | bytes 5120 | tf_op jit(solution)/shard_map/all_gather | solution.py:18
  250.1 0.6 convolution_bitcast_fusion
  251.1 2.3 multiply_reduce_fusion
  253.6 2.6 psum.7
  256.5 1.1 copy.43
  257.7 0.8 maximum_convert_fusion
  259.1 1.1 stack.18
  260.3 1.1 stack.17
  261.4 1.1 stack.16
  262.9 2.6 fusion.4
  266.4 59.5 %all-gather.21.cloned.1.call-done = bf16[512,2048]{1,0:T(8,128)(2,1)} async-done(((bf16[512,128]{1,0:T(8,128)(2,1)}), bf16[512,2048]{1,0:T(8,128)(2,1)}) %all-gather.21.cloned.1.call-update) | async-done | bytes 2097168 | tf_op jit(solution)/shard_map/all_gather | solution.py:168
  325.9 4.0 fusion.24
  329.9 59.8 %all-gather.25.cloned.1.call-done = bf16[512,2048]{1,0:T(8,128)(2,1)} async-done(((bf16[512,128]{1,0:T(8,128)(2,1)}), bf16[512,2048]{1,0:T(8,128)(2,1)}) %all-gather.25.cloned.1.call-update) | async-done | bytes 2097168 | tf_op jit(solution)/shard_map/all_gather | solution.py:169
  389.7 3.3 fusion
  393.1 6.7 %reduce-scatter.2.cloned.1.call-done = bf16[128,2048]{1,0:T(8,128)(2,1)} async-done(((bf16[256,2048]{1,0:T(8,128)(2,1)}), bf16[128,2048]{1,0:T(8,128)(2,1)}) %reduce-scatter.2.cloned.1.call-update) | async-done | bytes 524304 | tf_op jit(solution)/shard_map/reduce_scatter | solution.py:171
  (95 shorter events, 5.4 us)
Async XLA Ops:
  6.5 259.4 %copy-start = (bf16[4,256,256]{2,1,0:T(8,128)(2,1)S(1)}, bf16[4,256,256]{2,1,0:T(8,128)(2,1)}, u32[]{:S(2)}) copy-start(bf16[4,256,256]{2,1,0:T(8,128)(2,1)} %param.28) | copy-start | bytes 1572868
  6.5 25.5 %copy-start.6 = (bf16[128,512]{1,0:T(8,128)(2,1)S(1)}, bf16[128,512]{1,0:T(8,128)(2,1)}, u32[]{:S(2)}) copy-start(bf16[128,512]{1,0:T(8,128)(2,1)} %param.20) | copy-start | bytes 393220
  6.5 36.1 %copy-start.7 = (bf16[128,512]{1,0:T(8,128)(2,1)S(1)}, bf16[128,512]{1,0:T(8,128)(2,1)}, u32[]{:S(2)}) copy-start(bf16[128,512]{1,0:T(8,128)(2,1)} %param.22) | copy-start | bytes 393220
  6.5 59.1 %all-gather.27.cloned.1.call-start = ((), (), s32[]{:S(2)}) async-start(), calls=%async_computation.9 | async-start | bytes 1572864 | tf_op jit(solution)/shard_map/all_gather | solution.py:96
  7.3 61.8 %all-gather.17.cloned.1.call-start = ((), (), s32[]{:S(2)}) async-start(), calls=%async_computation.3 | async-start | bytes 2621440 | tf_op jit(solution)/shard_map/all_gather | solution.py:112
  20.5 32.6 %copy-start.8 = (bf16[128,512]{1,0:T(8,128)(2,1)S(1)}, bf16[128,512]{1,0:T(8,128)(2,1)}, u32[]{:S(2)}) copy-start(bf16[128,512]{1,0:T(8,128)(2,1)} %param.23) | copy-start | bytes 393220
  20.5 94.7 %all-gather.23.cloned.1.call-start = ((), (), s32[]{:S(2)}) async-start(), calls=%async_computation.6 | async-start | bytes 2621440 | tf_op jit(solution)/shard_map/all_gather | solution.py:115
  32.0 33.5 %copy-start.10 = (f32[1,256,4]{1,2,0:T(4,128)S(1)}, f32[1,256,4]{1,2,0:T(4,128)}, u32[]{:S(2)}) copy-start(f32[1,256,4]{1,2,0:T(4,128)} %param.26) | copy-start | bytes 12292
  32.0 129.1 %all-gather.15.cloned.1.call-start = ((), (), s32[]{:S(2)}) async-start(), calls=%async_computation.2 | async-start | bytes 2621440 | tf_op jit(solution)/shard_map/all_gather | solution.py:111
  42.6 26.5 %copy-start.15 = (f32[2048]{0:T(1024)S(1)}, f32[2048]{0:T(1024)}, u32[]{:S(2)}) copy-start(f32[2048]{0:T(1024)} %param.19) | copy-start | bytes 24580
  42.6 26.5 %copy-start.17 = (f32[512]{0:T(512)S(1)}, f32[512]{0:T(512)}, u32[]{:S(2)}) copy-start(f32[512]{0:T(512)} %param.25) | copy-start | bytes 6148
  42.6 164.4 %all-gather.13.cloned.1.call-start = ((), (), s32[]{:S(2)}) async-start(), calls=%async_computation.1 | async-start | bytes 2621440 | tf_op jit(solution)/shard_map/all_gather | solution.py:113
  53.1 213.4 %all-gather.19.cloned.1.call-start = ((), (), s32[]{:S(2)}) async-start(), calls=%async_computation.4 | async-start | bytes 2621440 | tf_op jit(solution)/shard_map/all_gather | solution.py:114
  63.1 262.7 %all-gather.21.cloned.1.call-start = ((), (), s32[]{:S(2)}) async-start(), calls=%async_computation.5 | async-start | bytes 2228224 | tf_op jit(solution)/shard_map/all_gather | solution.py:168
  63.9 325.9 %all-gather.25.cloned.1.call-start = ((), (), s32[]{:S(2)}) async-start(), calls=%async_computation.7 | async-start | bytes 2228224 | tf_op jit(solution)/shard_map/all_gather | solution.py:169
  64.6 335.2 %reduce-scatter.2.cloned.1.call-start = ((), (), s32[]{:S(2)}) async-start(), calls=%async_computation.8 | async-start | bytes 1572864 | tf_op jit(solution)/shard_map/reduce_scatter | solution.py:171
  67.2 139.8 %copy-start.12 = (f32[256]{0:T(256)}, f32[256]{0:T(256)S(1)}, u32[]{:S(2)}) copy-start(f32[256]{0:T(256)S(1)} %add_rsqrt_fusion.1) | copy-start | bytes 3076
  74.3 86.7 %copy-start.4 = (bf16[1,256,2048]{2,1,0:T(8,128)(2,1)S(1)}, bf16[1,256,2048]{2,1,0:T(8,128)(2,1)}, u32[]{:S(2)}) copy-start(bf16[1,256,2048]{2,1,0:T(8,128)(2,1)} %all-gather.27.cloned.1.call-done) | copy-start | bytes 3145732
  118.5 139.2 %collective-permute-start = (bf16[16,512]{1,0:T(8,128)(2,1)}, bf16[16,512]{1,0:T(8,128)(2,1)}, u32[]{:S(2)}, u32[]{:S(2)}) collective-permute-start(bf16[16,512]{1,0:T(8,128)(2,1)} %slice.57), channel_id=1, source_target_pairs={{0,8},{8,16},{16,24},{1,9},{9,17},{17,25},{2,10},{10,18},{18,26},{... | collective-permute-start | bytes 49160 | tf_op jit(solution)/shard_map/ppermute | solution.py:38
  214.3 25.7 %copy-start.9 = (f32[4,128]{1,0:T(4,128)S(1)}, f32[4,128]{1,0:T(4,128)}, u32[]{:S(2)}) copy-start(f32[4,128]{1,0:T(4,128)} %get-tuple-element.127) | copy-start | bytes 6148
  250.1 1.0 copy-start.1
  259.1 3.8 copy-start.14
  260.3 2.6 copy-start.2
  261.4 1.5 copy-start.3
  262.9 3.3 copy-start.11
  265.5 60.4 %copy-start.5 = (f32[4,64,4,128]{3,2,1,0:T(4,128)S(1)}, f32[4,64,4,128]{3,2,1,0:T(4,128)}, u32[]{:S(2)}) copy-start(f32[4,64,4,128]{3,2,1,0:T(4,128)} %copy.43) | copy-start | bytes 1572868
  265.5 60.4 %copy-start.13 = (f32[256]{0:T(256)S(1)}, f32[256]{0:T(256)}, u32[]{:S(2)}) copy-start(f32[256]{0:T(256)} %copy-done.12) | copy-start | bytes 3076
  265.5 60.4 %copy-start.16 = (f32[2048]{0:T(1024)S(1)}, f32[2048]{0:T(1024)}, u32[]{:S(2)}) copy-start(f32[2048]{0:T(1024)} %param.19) | copy-start | bytes 24580
Sparse Core Ops, SparseCore 0:
  8.9 11.7 all-gather.26
  22.2 46.8 all-gather.16
  70.7 44.4 all-gather.22
  116.6 44.4 all-gather.14
  162.5 44.4 all-gather.12
  208.4 52.9 all-gather.18
  264.1 61.7 all-gather.20
  328.6 61.1 all-gather.24
  393.2 6.5 reduce-scatter.1
where the time goes:
time: 407 us; the launch traced here: 406 us
  waiting for transfers between devices  252 us (62%)
  blocking collectives  90.1 us (22%)
  matrix products  24 us (6%)
  other arithmetic  13.8 us (3%)
  between operations  13.7 us (3%)
  local copies, waits for them, and re-layouts  9.22 us (2%)
    all_gather x1, waiting for transfers between devices, body(): lax.all_gather(w_out_pool, ('sp', 'fs'), axis=1, tiled=True)  59.8 us
    all_gather x1, waiting for transfers between devices, body(): lax.all_gather(recurrent_output_weight, ('sp', 'fs'), axis=1, tiled=True)  59.5 us
    all_gather x1, waiting for transfers between devices, body(): lax.all_gather(near_rows[2], 'sp', axis=0, tiled=True)  42.4 us
    all_gather x1, waiting for transfers between devices, body(): lax.all_gather(near_rows[4], 'sp', axis=0, tiled=True)  40.8 us
    all_gather x1, waiting for transfers between devices, body(): lax.all_gather(near_rows[0], 'sp', axis=0, tiled=True)  39 us
    all_gather x2, blocking collectives, carried_in(): lax.all_gather(a.astype(kind), axis)  32 us
    all_gather x1, blocking collectives, body(): lax.all_gather(forget_weight, 'fs', axis=0, tiled=True)  13.2 us
    all_gather x1, blocking collectives, body(): lax.all_gather(w_pool, 'fs', axis=0, tiled=True)  11.4 us
  transfers between devices with their start and end apart: 10, of which 7 were waited for; matrix products, arithmetic and copies ran while one was open for 11% of the time, Pallas kernels for 0%

commit v1 on v0

--- a/solution.py
+++ b/solution.py
@@ -2,6 +2,7 @@
 import jax.numpy as jnp
 from jax import lax
 from jax.sharding import PartitionSpec as P
+from jax.lax import all_gather
 
 HEAD_DIM = 128
 D_HGRN = 1024
@@ -93,6 +94,10 @@
     recurrent_output_weight,
     w_out_pool,
 ):
+
+    def mix_slots(page):
+        return jnp.concatenate(all_gather(page, ("sp", "fs")), 1)
+
     gathered = lax.all_gather(tokens[0], "tp", axis=1, tiled=True)
     features_f = gathered.astype(jnp.float32)
     token_scale = lax.rsqrt(jnp.mean(features_f * features_f, axis=-1, keepdims=True) + EPS)
@@ -165,7 +170,7 @@
     mapped = jnp.einsum("tcd,cde->tce", pooled, local_weight, preferred_element_type=jnp.float32)
     pool_out = (mapped.reshape(tok_rows, pool_dev) * pool_gain).astype(jnp.bfloat16)
     rec_columns, pool_columns = (
-        lax.all_gather(recurrent_output_weight, ("sp", "fs"), axis=1, tiled=True),
+        mix_slots(recurrent_output_weight),
         lax.all_gather(w_out_pool, ("sp", "fs"), axis=1, tiled=True),
     )
     mixed = lax.psum_scatter(

time: 407 us -> 398 us (0.978)
  waiting for transfers between devices: 252 us -> 245 us
  blocking collectives: 90.1 us -> 84.3 us
    all_gather x1, waiting for transfers between devices: 59.5 us -> 9.24 us  [mix_slots(): return jnp.concatenate(all_gather(page, ('sp', 'fs')), 1)]
    all_gather x1, waiting for transfers between devices: 0.02 us -> 42 us  [body(): lax.all_gather(near_rows[3], 'sp', axis=0, tiled=True)]
    all_gather x2, blocking collectives: 32 us -> 26.2 us  [carried_in(): lax.all_gather(a.astype(kind), axis)]
  transfers between devices with their start and end apart: 10 -> 10, of which waited for: 7 -> 8; matrix products, arithmetic and copies ran while one was open for 11% -> 12% of each run, Pallas kernels for 0% -> 0%
where the time goes in v1:
time: 398 us; the launch traced here: 397 us
  waiting for transfers between devices  245 us (62%)
  blocking collectives  84.3 us (21%)
  matrix products  24 us (6%)
  other arithmetic  13.8 us (3%)
  between operations  13.6 us (3%)
  local copies, waits for them, and re-layouts  13.2 us (3%)
    all_gather x1, waiting for transfers between devices, body(): lax.all_gather(w_out_pool, ('sp', 'fs'), axis=1, tiled=True)  60.5 us
    all_gather x1, waiting for transfers between devices, body(): lax.all_gather(near_rows[2], 'sp', axis=0, tiled=True)  42.4 us
    all_gather x1, waiting for transfers between devices, body(): lax.all_gather(near_rows[3], 'sp', axis=0, tiled=True)  42 us
    all_gather x1, waiting for transfers between devices, body(): lax.all_gather(near_rows[4], 'sp', axis=0, tiled=True)  40.8 us
    all_gather x1, waiting for transfers between devices, body(): lax.all_gather(near_rows[0], 'sp', axis=0, tiled=True)  39 us
    all_gather x2, blocking collectives, carried_in(): lax.all_gather(a.astype(kind), axis)  26.2 us
    all_gather x1, blocking collectives, body(): lax.all_gather(forget_weight, 'fs', axis=0, tiled=True)  13.2 us
    all_gather x1, blocking collectives, body(): lax.all_gather(w_pool, 'fs', axis=0, tiled=True)  11.4 us
  transfers between devices with their start and end apart: 10, of which 8 were waited for; matrix products, arithmetic and copies ran while one was open for 12% of the time, Pallas kernels for 0%

profile of v1, /device:TPU:0, one launch (start us, length us, event | category | flops | bytes accessed | tf_op | source)
XLA Modules:
  0.0 396.8 jit_solution(11256586523641989647)
XLA Ops:
  6.5 0.7 all-gather.26.cloned.1.call-update
  7.3 13.2 %all_gather.57 = bf16[512,512]{1,0:T(8,128)(2,1)} all-gather(bf16[128,512]{1,0:T(8,128)(2,1)} %param.21), channel_id=1, replica_groups=mesh['sp'=4,'fs'=4,'tp'=2] {'fs'}, dimensions={0}, use_global_device_ids=true | all-gather | bytes 655360 | tf_op jit(solution)/shard_map/all_gather | solution.py:110
  20.6 11.4 %all_gather.66 = bf16[512,512]{1,0:T(8,128)(2,1)} all-gather(bf16[128,512]{1,0:T(8,128)(2,1)} %param.24), channel_id=1, replica_groups=mesh['sp'=4,'fs'=4,'tp'=2] {'fs'}, dimensions={0}, use_global_device_ids=true | all-gather | bytes 655360 | tf_op jit(solution)/shard_map/all_gather | solution.py:113
  32.1 10.5 %all_gather.55 = bf16[512,512]{1,0:T(8,128)(2,1)} all-gather(bf16[128,512]{1,0:T(8,128)(2,1)S(1)} %copy-done.6), channel_id=1, replica_groups=mesh['sp'=4,'fs'=4,'tp'=2] {'fs'}, dimensions={0}, use_global_device_ids=true | all-gather | bytes 655360 | tf_op jit(solution)/shard_map/all_gather | solution.py:109
  42.7 10.4 %all_gather.53 = bf16[512,512]{1,0:T(8,128)(2,1)} all-gather(bf16[128,512]{1,0:T(8,128)(2,1)S(1)} %copy-done.7), channel_id=1, replica_groups=mesh['sp'=4,'fs'=4,'tp'=2] {'fs'}, dimensions={0}, use_global_device_ids=true | all-gather | bytes 655360 | tf_op jit(solution)/shard_map/all_gather | solution.py:111
  53.7 10.1 %all_gather.62 = bf16[512,512]{1,0:T(8,128)(2,1)} all-gather(bf16[128,512]{1,0:T(8,128)(2,1)S(1)} %copy-done.8), channel_id=1, replica_groups=mesh['sp'=4,'fs'=4,'tp'=2] {'fs'}, dimensions={0}, use_global_device_ids=true | all-gather | bytes 655360 | tf_op jit(solution)/shard_map/all_gather | solution.py:112
  63.8 0.7 all-gather.24.cloned.1.call-update
  65.5 1.5 fusion.1
  67.1 2.0 all-gather.18.cloned.1.call-done
  69.1 2.9 negate_log-plus-one_fusion
  72.6 1.2 slice_bitcast_fusion
  73.7 0.6 fusion.15
  74.4 40.8 %all-gather.22.cloned.1.call-done = bf16[2048,512]{1,0:T(8,128)(2,1)} async-done(((bf16[512,512]{1,0:T(8,128)(2,1)}), bf16[2048,512]{1,0:T(8,128)(2,1)}) %all-gather.22.cloned.1.call-update) | async-done | bytes 2097168 | tf_op jit(solution)/shard_map/all_gather | solution.py:120
  115.2 2.7 convolution_convert_fusion
  117.9 0.6 slice.57
  118.5 2.7 collective-permute-start
  121.1 1.0 reshape_reshape.11
  122.1 39.0 %all-gather.16.cloned.1.call-done = bf16[2048,512]{1,0:T(8,128)(2,1)} async-done(((bf16[512,512]{1,0:T(8,128)(2,1)}), bf16[2048,512]{1,0:T(8,128)(2,1)}) %all-gather.16.cloned.1.call-update) | async-done | bytes 2097168 | tf_op jit(solution)/shard_map/all_gather | solution.py:116
  161.1 2.4 divide_multiply_fusion
  163.5 1.0 reshape_reshape.10
  164.6 42.4 %all-gather.14.cloned.1.call-done = bf16[2048,512]{1,0:T(8,128)(2,1)} async-done(((bf16[512,512]{1,0:T(8,128)(2,1)}), bf16[2048,512]{1,0:T(8,128)(2,1)}) %all-gather.14.cloned.1.call-update) | async-done | bytes 2097168 | tf_op jit(solution)/shard_map/all_gather | solution.py:118
  207.0 2.3 convolution_convert_fusion.4
  209.4 1.7 exponential_multiply_fusion.1
  211.1 1.0 convolution_select_fusion
  212.1 1.2 fusion.39
  213.3 1.0 fusion.21
  214.3 3.7 while.26
  214.3 0.7 bitcast_dynamic-update-slice_fusion.2
  215.2 0.7 bitcast_dynamic-update-slice_fusion.2
  216.2 0.7 bitcast_dynamic-update-slice_fusion.2
  217.1 0.7 bitcast_dynamic-update-slice_fusion.2
  218.0 16.4 %all-gather.2 = bf16[16,128,128]{2,1,0:T(8,128)(2,1)S(1)} all-gather(bf16[4,128,128]{2,1,0:T(8,128)(2,1)S(1)} %convert_element_type.97), channel_id=4, replica_groups=mesh['sp'=4,'fs'=4,'tp'=2] {'sp'}, dimensions={0}, use_global_device_ids=true | all-gather | bytes 655360 | tf_op jit(solution)/shard_map/all_gather | solution.py:19
  234.5 9.7 %all-gather.4 = bf16[4,4,128]{2,1,0:T(4,128)(2,1)S(1)} all-gather(bf16[1,4,128]{2,1,0:T(4,128)(2,1)S(1)} %fusion.42), channel_id=3, replica_groups=mesh['sp'=4,'fs'=4,'tp'=2] {'sp'}, dimensions={0}, use_global_device_ids=true | all-gather | bytes 5120 | tf_op jit(solution)/shard_map/all_gather | solution.py:19
  245.2 2.3 multiply_reduce_fusion
  247.7 2.6 psum.7
  250.6 1.1 copy.67
  251.8 0.8 maximum_convert_fusion
  253.2 1.1 stack.18
  254.4 1.1 stack.17
  255.5 1.1 stack.16
  257.0 2.6 fusion.4
  260.4 9.2 %all-gather.28.cloned.1.call-done = bf16[8192,128]{1,0:T(8,128)(2,1)} async-done(((bf16[512,128]{1,0:T(8,128)(2,1)}), bf16[8192,128]{1,0:T(8,128)(2,1)}) %all-gather.28.cloned.1.call-update) | async-done | bytes 2097168 | tf_op jit(solution)/shard_map/all_gather | solution.py:99
  269.7 4.0 %copy.68 = bf16[512,16,128]{0,2,1:T(8,128)(2,1)} copy(bf16[512,16,128]{2,0,1:T(8,128)(2,1)} %bitcast.87) | data formatting | bytes 4194304 | tf_op jit(solution)/shard_map/reshape | solution.py:99
  273.7 42.0 %all-gather.20.cloned.1.call-done = bf16[2048,512]{1,0:T(8,128)(2,1)} async-done(((bf16[512,512]{1,0:T(8,128)(2,1)}), bf16[2048,512]{1,0:T(8,128)(2,1)}) %all-gather.20.cloned.1.call-update) | async-done | bytes 2097168 | tf_op jit(solution)/shard_map/all_gather | solution.py:119
  315.8 4.0 %fusion.24 = f32[256,2048]{1,0:T(8,128)S(1)} fusion(bf16[512,2048]{0,1:T(8,128)(2,1)} %bitcast.88, f32[32,8,4,128]{3,2,1,0:T(4,128)S(1)} %bitcast.90, bf16[2048,512]{1,0:T(8,128)(2,1)} %all-gather.20.cloned.1.call-done, f32[512]{0:T(512)S(1)} %copy-done.18, f32[256]{0:T(256)S(1)} %add_rsqrt_fusion, bf16[1,256,2048]{2,1,0:T(8,128)(2,1)} %all-gather.26.cloned.1.call-done, ...), kind=kOutput, calls=%fused_computation.49 | convolution fusion | flops 1077149696 | bytes 7876608 | tf_op jit(solution)/shard_map/dot_general | solution.py:178
  319.8 60.5 %all-gather.24.cloned.1.call-done = bf16[512,2048]{1,0:T(8,128)(2,1)} async-done(((bf16[512,128]{1,0:T(8,128)(2,1)}), bf16[512,2048]{1,0:T(8,128)(2,1)}) %all-gather.24.cloned.1.call-update) | async-done | bytes 2097168 | tf_op jit(solution)/shard_map/all_gather | solution.py:174
  380.2 3.3 fusion
  383.6 6.7 %reduce-scatter.2.cloned.1.call-done = bf16[128,2048]{1,0:T(8,128)(2,1)} async-done(((bf16[256,2048]{1,0:T(8,128)(2,1)}), bf16[128,2048]{1,0:T(8,128)(2,1)}) %reduce-scatter.2.cloned.1.call-update) | async-done | bytes 524304 | tf_op jit(solution)/shard_map/reduce_scatter | solution.py:176
  (98 shorter events, 6.4 us)
Async XLA Ops:
  6.5 253.5 %copy-start = (bf16[4,256,256]{2,1,0:T(8,128)(2,1)S(1)}, bf16[4,256,256]{2,1,0:T(8,128)(2,1)}, u32[]{:S(2)}) copy-start(bf16[4,256,256]{2,1,0:T(8,128)(2,1)} %param.28) | copy-start | bytes 1572868
  6.5 25.5 %copy-start.6 = (bf16[128,512]{1,0:T(8,128)(2,1)S(1)}, bf16[128,512]{1,0:T(8,128)(2,1)}, u32[]{:S(2)}) copy-start(bf16[128,512]{1,0:T(8,128)(2,1)} %param.20) | copy-start | bytes 393220
  6.5 36.1 %copy-start.7 = (bf16[128,512]{1,0:T(8,128)(2,1)S(1)}, bf16[128,512]{1,0:T(8,128)(2,1)}, u32[]{:S(2)}) copy-start(bf16[128,512]{1,0:T(8,128)(2,1)} %param.22) | copy-start | bytes 393220
  6.5 59.0 %all-gather.26.cloned.1.call-start = ((), (), s32[]{:S(2)}) async-start(), calls=%async_computation.8 | async-start | bytes 1572864 | tf_op jit(solution)/shard_map/all_gather | solution.py:101
  7.3 61.8 %all-gather.18.cloned.1.call-start = ((), (), s32[]{:S(2)}) async-start(), calls=%async_computation.3 | async-start | bytes 2621440 | tf_op jit(solution)/shard_map/all_gather | solution.py:117
  20.5 33.2 %copy-start.8 = (bf16[128,512]{1,0:T(8,128)(2,1)S(1)}, bf16[128,512]{1,0:T(8,128)(2,1)}, u32[]{:S(2)}) copy-start(bf16[128,512]{1,0:T(8,128)(2,1)} %param.23) | copy-start | bytes 393220
  20.5 94.7 %all-gather.22.cloned.1.call-start = ((), (), s32[]{:S(2)}) async-start(), calls=%async_computation.5 | async-start | bytes 2621440 | tf_op jit(solution)/shard_map/all_gather | solution.py:120
  32.0 33.4 %copy-start.10 = (f32[1,256,4]{1,2,0:T(4,128)S(1)}, f32[1,256,4]{1,2,0:T(4,128)}, u32[]{:S(2)}) copy-start(f32[1,256,4]{1,2,0:T(4,128)} %param.26) | copy-start | bytes 12292
  32.0 129.1 %all-gather.16.cloned.1.call-start = ((), (), s32[]{:S(2)}) async-start(), calls=%async_computation.2 | async-start | bytes 2621440 | tf_op jit(solution)/shard_map/all_gather | solution.py:116
  42.6 26.5 %copy-start.15 = (f32[2048]{0:T(1024)S(1)}, f32[2048]{0:T(1024)}, u32[]{:S(2)}) copy-start(f32[2048]{0:T(1024)} %param.19) | copy-start | bytes 24580
  42.6 26.5 %copy-start.17 = (f32[512]{0:T(512)S(1)}, f32[512]{0:T(512)}, u32[]{:S(2)}) copy-start(f32[512]{0:T(512)} %param.25) | copy-start | bytes 6148
  42.6 164.4 %all-gather.14.cloned.1.call-start = ((), (), s32[]{:S(2)}) async-start(), calls=%async_computation.1 | async-start | bytes 2621440 | tf_op jit(solution)/shard_map/all_gather | solution.py:118
  53.0 216.6 %all-gather.28.cloned.1.call-start = ((), (), s32[]{:S(2)}) async-start(), calls=%async_computation.9 | async-start | bytes 2228224 | tf_op jit(solution)/shard_map/all_gather | solution.py:99
  53.6 262.1 %all-gather.20.cloned.1.call-start = ((), (), s32[]{:S(2)}) async-start(), calls=%async_computation.4 | async-start | bytes 2621440 | tf_op jit(solution)/shard_map/all_gather | solution.py:119
  63.8 316.4 %all-gather.24.cloned.1.call-start = ((), (), s32[]{:S(2)}) async-start(), calls=%async_computation.6 | async-start | bytes 2228224 | tf_op jit(solution)/shard_map/all_gather | solution.py:174
  64.5 325.8 %reduce-scatter.2.cloned.1.call-start = ((), (), s32[]{:S(2)}) async-start(), calls=%async_computation.7 | async-start | bytes 1572864 | tf_op jit(solution)/shard_map/reduce_scatter | solution.py:176
  67.1 139.9 %copy-start.12 = (f32[256]{0:T(256)}, f32[256]{0:T(256)S(1)}, u32[]{:S(2)}) copy-start(f32[256]{0:T(256)S(1)} %add_rsqrt_fusion.1) | copy-start | bytes 3076
  74.4 86.7 %copy-start.4 = (bf16[1,256,2048]{2,1,0:T(8,128)(2,1)S(1)}, bf16[1,256,2048]{2,1,0:T(8,128)(2,1)}, u32[]{:S(2)}) copy-start(bf16[1,256,2048]{2,1,0:T(8,128)(2,1)} %all-gather.26.cloned.1.call-done) | copy-start | bytes 3145732
  118.5 133.3 %collective-permute-start = (bf16[16,512]{1,0:T(8,128)(2,1)}, bf16[16,512]{1,0:T(8,128)(2,1)}, u32[]{:S(2)}, u32[]{:S(2)}) collective-permute-start(bf16[16,512]{1,0:T(8,128)(2,1)} %slice.57), channel_id=1, source_target_pairs={{0,8},{8,16},{16,24},{1,9},{9,17},{17,25},{2,10},{10,18},{18,26},{... | collective-permute-start | bytes 49160 | tf_op jit(solution)/shard_map/ppermute | solution.py:39
  214.3 20.2 %copy-start.9 = (f32[4,128]{1,0:T(4,128)S(1)}, f32[4,128]{1,0:T(4,128)}, u32[]{:S(2)}) copy-start(f32[4,128]{1,0:T(4,128)} %get-tuple-element.127) | copy-start | bytes 6148
  244.2 1.0 copy-start.1
  253.2 3.7 copy-start.14
  254.4 2.6 copy-start.2
  255.5 1.5 copy-start.3
  257.0 3.3 copy-start.11
  269.7 46.1 %copy-start.5 = (f32[4,64,4,128]{3,2,1,0:T(4,128)S(1)}, f32[4,64,4,128]{3,2,1,0:T(4,128)}, u32[]{:S(2)}) copy-start(f32[4,64,4,128]{3,2,1,0:T(4,128)} %copy.67) | copy-start | bytes 1572868
  269.7 46.1 %copy-start.13 = (f32[256]{0:T(256)S(1)}, f32[256]{0:T(256)}, u32[]{:S(2)}) copy-start(f32[256]{0:T(256)} %copy-done.12) | copy-start | bytes 3076
  269.7 46.1 %copy-start.16 = (f32[2048]{0:T(1024)S(1)}, f32[2048]{0:T(1024)}, u32[]{:S(2)}) copy-start(f32[2048]{0:T(1024)} %param.19) | copy-start | bytes 24580
  269.7 46.1 %copy-start.18 = (f32[512]{0:T(512)S(1)}, f32[512]{0:T(512)}, u32[]{:S(2)}) copy-start(f32[512]{0:T(512)} %param.27) | copy-start | bytes 6148
Sparse Core Ops, SparseCore 0:
  8.9 11.7 all-gather.25
  22.2 46.8 all-gather.17
  70.7 44.4 all-gather.21
  116.6 44.4 all-gather.15
  162.5 44.4 all-gather.13
  209.6 60.0 all-gather.27
  271.3 44.4 all-gather.19
  318.4 61.7 all-gather.23
  383.7 6.5 reduce-scatter.1
